TPU v7x, 32 devices: a whole 2x2x4 slice. The times are simulated.
32 devices in a mesh: fs: 8 (over z, y), tp: 4 (over x, core).
Axes of the slice: x: 2, y: 2, z: 4, core: 2. Of those that a mesh axis runs over, the one named last changes fastest.
Arguments:
- tokens: bfloat16 [640, 3072], P('tp'), may hold values from -6 to 6
- gain_first: float32 [3072], replicated, may hold values from 0.1 to 1.9
- gain_second: float32 [3072], replicated, may hold values from 0.1 to 1.9
- gate_first: float32 [3072, 8192], P('fs', 'tp'), may hold values from -0.109375 to 0.109375
- up_first: float32 [3072, 8192], P('fs', 'tp'), may hold values from -0.109375 to 0.109375
- down_first: float32 [8192, 3072], P('fs', 'tp'), may hold values from -0.09375 to 0.09375
- gate_second: float32 [3072, 8192], P('fs', 'tp'), may hold values from -0.109375 to 0.109375
- up_second: float32 [3072, 8192], P('fs', 'tp'), may hold values from -0.109375 to 0.109375
- down_second: float32 [8192, 3072], P('fs', 'tp'), may hold values from -0.09375 to 0.09375
Outputs:
- result_rows: bfloat16 [640, 3072], P('tp')
- serve_gate_first: bfloat16 [3072, 8192], P(None, 'fs')
- serve_up_first: bfloat16 [3072, 8192], P(None, 'fs')
- serve_down_first: bfloat16 [8192, 3072], P('fs')
- serve_gate_second: bfloat16 [3072, 8192], P(None, 'fs')
- serve_up_second: bfloat16 [3072, 8192], P(None, 'fs')
- serve_down_second: bfloat16 [8192, 3072], P('fs')
All inputs are finite; a program needn't handle non-finite values.
Results may differ from a plain program's by a relative error of at most 0.011.
Values may be sent and summed in bfloat16 or wider, within the bound.
A program may use at most 192 MiB of HBM per device.

v0:
```python
import jax
import jax.numpy as jnp
from jax import lax
from jax.sharding import PartitionSpec as P


def plain_norm(values):
    values = values.astype(jnp.float32)
    center = jnp.mean(values, axis=-1, keepdims=True)
    spread = jnp.mean(jnp.square(values - center), axis=-1, keepdims=True)
    return (values - center) * lax.rsqrt(spread + 1e-05)


def sum_over_hidden(partial_value):
    pieces = lax.all_to_all(
        partial_value.astype(jnp.bfloat16), "fs", split_axis=1, concat_axis=0, tiled=True
    )
    rows = partial_value.shape[0]
    pieces = pieces.reshape(-1, rows, pieces.shape[1]).astype(jnp.float32)
    summed = jnp.sum(pieces, axis=0).astype(jnp.bfloat16)
    return lax.all_gather(summed, "fs", axis=1, tiled=True).astype(jnp.float32)


def regroup(folded):
    spread = lax.all_to_all(folded, "tp", split_axis=0, concat_axis=1, tiled=True)
    parts = lax.axis_size("fs")
    rows = spread.shape[0]
    owned = lax.all_to_all(spread, "fs", split_axis=1, concat_axis=0, tiled=True)
    owned = owned.reshape(parts, rows, owned.shape[1])
    whole = lax.all_gather(owned, "tp", axis=1, tiled=True)
    return whole.reshape(-1, whole.shape[2])


def half_step(normed, scales, w_gate, w_rising, w_down):
    gate_part = jnp.dot(normed, w_gate, preferred_element_type=jnp.float32)
    rising = jnp.dot(normed, w_rising, preferred_element_type=jnp.float32)
    hidden = (jax.nn.silu(gate_part) * rising).astype(jnp.bfloat16)
    partial_value = jnp.dot(hidden, w_down, preferred_element_type=jnp.float32)
    block = sum_over_hidden(partial_value)
    mixed = 1.6817928 * scales[None, :] * normed.astype(jnp.float32) + 0.5 * block
    return plain_norm(mixed).astype(jnp.bfloat16)


def on_device(
    tokens,
    gain_first,
    gain_second,
    gate_first,
    up_first,
    down_first,
    gate_second,
    up_second,
    down_second,
):
    row_count = gate_first.shape[0]
    offset = lax.axis_index("fs") * row_count

    def fold_gain(weight, scales):
        picked = lax.dynamic_slice_in_dim(scales, offset, row_count, 0)
        return (picked[:, None] * weight).astype(jnp.bfloat16)

    serve_gate_first = regroup(fold_gain(gate_first, gain_first))
    serve_up_first = regroup(fold_gain(up_first, gain_first))
    serve_down_first = lax.all_gather(down_first.astype(jnp.bfloat16), "tp", axis=1, tiled=True)
    serve_gate_second = regroup(fold_gain(gate_second, gain_second))
    serve_up_second = regroup(fold_gain(up_second, gain_second))
    serve_down_second = lax.all_gather(down_second.astype(jnp.bfloat16), "tp", axis=1, tiled=True)
    normed_zero = plain_norm(tokens).astype(jnp.bfloat16)
    normed_one = half_step(
        normed_zero, gain_first, serve_gate_first, serve_up_first, serve_down_first
    )
    result_rows = half_step(
        normed_one, gain_second, serve_gate_second, serve_up_second, serve_down_second
    )
    return (
        result_rows,
        serve_gate_first,
        serve_up_first,
        serve_down_first,
        serve_gate_second,
        serve_up_second,
        serve_down_second,
    )


def solution(mesh):
    placed = (
        P("tp", None),
        P(),
        P(),
        P("fs", "tp"),
        P("fs", "tp"),
        P("fs", "tp"),
        P("fs", "tp"),
        P("fs", "tp"),
        P("fs", "tp"),
    )
    return jax.shard_map(
        on_device,
        mesh=mesh,
        in_specs=placed,
        out_specs=(
            P("tp", None),
            P(None, "fs"),
            P(None, "fs"),
            P("fs", None),
            P(None, "fs"),
            P(None, "fs"),
            P("fs", None),
        ),
        check_vma=False,
    )
```

profile of v0, /device:TPU:0, one launch (start us, length us, event | category | flops | bytes accessed | tf_op | source)
XLA Modules:
  0.0 523.0 jit_solution(2696292961990616382)
XLA Ops:
  8.0 3.7 multiply_convert_fusion.3
  11.7 24.1 %all_to_all.154 = bf16[4,96,2048]{2,1,0:T(8,128)(2,1)S(1)} all-to-all(bf16[4,96,2048]{2,1,0:T(8,128)(2,1)S(1)} %bitcast.44), channel_id=1, replica_groups=mesh['fs'=8,'tp'=4] {'tp'}, dimensions={0} | all-to-all | bytes 3145728 | tf_op jit(solution)/shard_map/all_to_all | solution.py:25
  37.0 1.8 all_to_all.119
  38.9 2.3 copy.29
  41.2 42.3 %all_to_all.155 = bf16[96,8,1024]{2,0,1:T(8,128)(2,1)S(1)} all-to-all(bf16[96,8,1024]{2,0,1:T(8,128)(2,1)S(1)} %copy.29), channel_id=1, replica_groups=mesh['fs'=8,'tp'=4] {'fs'}, dimensions={1} | all-to-all | bytes 3145728 | tf_op jit(solution)/shard_map/all_to_all | solution.py:28
  83.5 2.0 copy.30
  85.6 36.1 %all_to_all.156 = bf16[4,96,2048]{2,1,0:T(8,128)(2,1)S(1)} all-to-all(bf16[4,96,2048]{2,1,0:T(8,128)(2,1)S(1)} %bitcast.42), channel_id=1, replica_groups=mesh['fs'=8,'tp'=4] {'tp'}, dimensions={0} | all-to-all | bytes 3145728 | tf_op jit(solution)/shard_map/all_to_all | solution.py:25
  124.2 39.1 %all_to_all.157 = bf16[96,8,1024]{2,0,1:T(8,128)(2,1)S(1)} all-to-all(bf16[96,8,1024]{2,0,1:T(8,128)(2,1)S(1)} %copy.33), channel_id=1, replica_groups=mesh['fs'=8,'tp'=4] {'fs'}, dimensions={1} | all-to-all | bytes 3145728 | tf_op jit(solution)/shard_map/all_to_all | solution.py:28
  163.3 2.0 copy.34
  166.8 3.9 multiply_convert_fusion.1
  170.7 39.8 %all_to_all.158 = bf16[4,96,2048]{2,1,0:T(8,128)(2,1)S(1)} all-to-all(bf16[4,96,2048]{2,1,0:T(8,128)(2,1)S(1)} %bitcast.45), channel_id=1, replica_groups=mesh['fs'=8,'tp'=4] {'tp'}, dimensions={0} | all-to-all | bytes 3145728 | tf_op jit(solution)/shard_map/all_to_all | solution.py:25
  211.7 1.8 all_to_all.133
  213.6 2.3 copy.38
  215.8 51.1 %all_to_all.159 = bf16[96,8,1024]{2,0,1:T(8,128)(2,1)S(1)} all-to-all(bf16[96,8,1024]{2,0,1:T(8,128)(2,1)S(1)} %copy.38), channel_id=1, replica_groups=mesh['fs'=8,'tp'=4] {'fs'}, dimensions={1} | all-to-all | bytes 3145728 | tf_op jit(solution)/shard_map/all_to_all | solution.py:28
  266.9 2.0 copy.39
  269.0 26.1 %all_to_all.160 = bf16[4,96,2048]{2,1,0:T(8,128)(2,1)S(1)} all-to-all(bf16[4,96,2048]{2,1,0:T(8,128)(2,1)S(1)} %bitcast.43), channel_id=1, replica_groups=mesh['fs'=8,'tp'=4] {'tp'}, dimensions={0} | all-to-all | bytes 3145728 | tf_op jit(solution)/shard_map/all_to_all | solution.py:25
  297.6 39.2 %all_to_all.161 = bf16[96,8,1024]{2,0,1:T(8,128)(2,1)S(1)} all-to-all(bf16[96,8,1024]{2,0,1:T(8,128)(2,1)S(1)} %copy.42), channel_id=1, replica_groups=mesh['fs'=8,'tp'=4] {'fs'}, dimensions={1} | all-to-all | bytes 3145728 | tf_op jit(solution)/shard_map/all_to_all | solution.py:28
  336.8 2.0 copy.43
  342.0 9.7 %copy.31 = bf16[8,384,1024]{2,1,0:T(8,128)(2,1)} copy(bf16[8,384,1024]{2,0,1:T(8,128)(2,1)} %all-gather.7.cloned.1.call-done) | data formatting | bytes 12582912 | tf_op jit(solution)/shard_map/all_gather | solution.py:30
  351.7 9.2 %copy.35 = bf16[8,384,1024]{2,1,0:T(8,128)(2,1)} copy(bf16[8,384,1024]{2,0,1:T(8,128)(2,1)} %all-gather.9.cloned.1.call-done) | data formatting | bytes 12582912 | tf_op jit(solution)/shard_map/all_gather | solution.py:30
  362.3 7.0 %convolution_convert_fusion.1 = bf16[160,3072]{1,0:T(8,128)(2,1)S(1)} fusion(bf16[1024,3072]{1,0:T(8,128)(2,1)} %all-gather.11.cloned.1.call-done, bf16[3072,1024]{1,0:T(8,128)(2,1)} %bitcast.38, f32[160,1024]{1,0:T(8,128)S(1)} %fusion.14, bf16[160,3072]{1,0:T(8,128)(2,1)S(1)} %copy-done.1, f32[160]{0:T(256)S(1)} %add_rsqrt_fusion.2, ...), kind=kOutput, calls=%fused_computation.1 | convolution fusion | flops 2016706560 | bytes 15205632 | tf_op jit(solution)/shard_map/dot_general | solution.py:38
  370.3 3.8 all-to-all-start.4
  374.1 9.1 %copy.40 = bf16[8,384,1024]{2,1,0:T(8,128)(2,1)} copy(bf16[8,384,1024]{2,0,1:T(8,128)(2,1)} %all-gather.13.cloned.1.call-done) | data formatting | bytes 12582912 | tf_op jit(solution)/shard_map/all_gather | solution.py:30
  383.7 9.0 %copy.44 = bf16[8,384,1024]{2,1,0:T(8,128)(2,1)} copy(bf16[8,384,1024]{2,0,1:T(8,128)(2,1)} %all-gather.15.cloned.1.call-done) | data formatting | bytes 12582912 | tf_op jit(solution)/shard_map/all_gather | solution.py:30
  392.7 5.5 %all-to-all-done.4 = bf16[160,8,384]{2,0,1:T(8,128)(2,1)S(1)} async-done(((bf16[160,8,384]{2,0,1:T(8,128)(2,1)}), bf16[160,8,384]{2,0,1:T(8,128)(2,1)S(1)}, u32[]{:S(2)}, u32[]{:S(2)}) %all-to-all-start.4) | async-done | bytes 983072 | tf_op jit(solution)/shard_map/all_to_all | solution.py:15
  398.3 33.7 %all_gather.27 = bf16[160,3072]{1,0:T(8,128)(2,1)S(1)} all-gather(bf16[160,384]{1,0:T(8,128)(2,1)S(1)} %reduce_sum.80), channel_id=1, replica_groups=mesh['fs'=8,'tp'=4] {'fs'}, dimensions={1}, use_global_device_ids=true | all-gather | bytes 1105920 | tf_op jit(solution)/shard_map/all_gather | solution.py:21
  436.0 6.9 %convolution_convert_fusion = bf16[160,3072]{1,0:T(8,128)(2,1)S(1)} fusion(bf16[1024,3072]{1,0:T(8,128)(2,1)} %all-gather.17.cloned.1.call-done, bf16[160,3072]{1,0:T(8,128)(2,1)S(1)} %multiply_convert_fusion.5, bf16[3072,1024]{1,0:T(8,128)(2,1)} %bitcast.40, f32[160,1024]{1,0:T(8,128)S(1)} %fusion.16), kind=kOutput, calls=%fused_computation | convolution fusion | flops 2014740480 | bytes 15204352 | tf_op jit(solution)/shard_map/dot_general | solution.py:38
  444.0 3.6 all-to-all-start.9
  447.6 23.0 %all-to-all-done.9 = bf16[160,8,384]{2,0,1:T(8,128)(2,1)S(1)} async-done(((bf16[160,8,384]{2,0,1:T(8,128)(2,1)}), bf16[160,8,384]{2,0,1:T(8,128)(2,1)S(1)}, u32[]{:S(2)}, u32[]{:S(2)}) %all-to-all-start.9) | async-done | bytes 983072 | tf_op jit(solution)/shard_map/all_to_all | solution.py:15
  470.6 33.6 %all_gather.31 = bf16[160,3072]{1,0:T(8,128)(2,1)S(1)} all-gather(bf16[160,384]{1,0:T(8,128)(2,1)S(1)} %reduce_sum.83), channel_id=1, replica_groups=mesh['fs'=8,'tp'=4] {'fs'}, dimensions={1}, use_global_device_ids=true | all-gather | bytes 1105920 | tf_op jit(solution)/shard_map/all_gather | solution.py:21
  506.9 6.1 %copy.54 = bf16[1024,3072]{1,0:T(8,128)(2,1)} copy(bf16[1024,3072]{1,0:T(8,128)(2,1)} %all-gather.11.cloned.1.call-done) | data formatting | bytes 12582912
  513.0 2.7 copy.55
  (71 shorter events, 23.9 us)
Async XLA Ops:
  7.2 334.9 %all-gather.7.cloned.1.call-start = ((), (), s32[]{:S(2)}) async-start(), calls=%async_computation.10 | async-start | bytes 7864320 | tf_op jit(solution)/shard_map/all_gather | solution.py:30
  85.5 266.2 %all-gather.9.cloned.1.call-start = ((), (), s32[]{:S(2)}) async-start(), calls=%async_computation.11 | async-start | bytes 7864320 | tf_op jit(solution)/shard_map/all_gather | solution.py:30
  163.3 2.1 copy-start.3
  165.3 1.4 copy-start.6
  165.3 196.9 %all-gather.11.cloned.1.call-start = ((), (), s32[]{:S(2)}) async-start(), calls=%async_computation.12 | async-start | bytes 7864320 | tf_op jit(solution)/shard_map/all_gather | solution.py:64
  166.7 207.4 %all-gather.13.cloned.1.call-start = ((), (), s32[]{:S(2)}) async-start(), calls=%async_computation.13 | async-start | bytes 7864320 | tf_op jit(solution)/shard_map/all_gather | solution.py:30
  269.0 114.7 %all-gather.15.cloned.1.call-start = ((), (), s32[]{:S(2)}) async-start(), calls=%async_computation.14 | async-start | bytes 7864320 | tf_op jit(solution)/shard_map/all_gather | solution.py:30
  336.8 2.1 copy-start.4
  338.8 97.2 %all-gather.17.cloned.1.call-start = ((), (), s32[]{:S(2)}) async-start(), calls=%async_computation.15 | async-start | bytes 7864320 | tf_op jit(solution)/shard_map/all_gather | solution.py:67
  340.2 1.2 copy-start.1
  351.7 9.2 %copy-start.2 = (bf16[8,384,1024]{2,1,0:T(8,128)(2,1)S(1)}, bf16[8,384,1024]{2,1,0:T(8,128)(2,1)}, u32[]{:S(2)}) copy-start(bf16[8,384,1024]{2,1,0:T(8,128)(2,1)} %copy.31) | copy-start | bytes 18874372
  369.3 4.8 copy-start.5
  370.3 27.8 %all-to-all-start.4 = ((bf16[160,8,384]{2,0,1:T(8,128)(2,1)}), bf16[160,8,384]{2,0,1:T(8,128)(2,1)S(1)}, u32[]{:S(2)}, u32[]{:S(2)}) async-start(bf16[160,8,384]{2,0,1:T(8,128)(2,1)} %bitcast.31), calls=%async_computation.4 | async-start | bytes 1966080 | tf_op jit(solution)/shard_map/all_to_all | solution.py:15
  432.0 2.8 copy-start
  444.0 26.5 %all-to-all-start.9 = ((bf16[160,8,384]{2,0,1:T(8,128)(2,1)}), bf16[160,8,384]{2,0,1:T(8,128)(2,1)S(1)}, u32[]{:S(2)}, u32[]{:S(2)}) async-start(bf16[160,8,384]{2,0,1:T(8,128)(2,1)} %bitcast.30), calls=%async_computation.9 | async-start | bytes 1966080 | tf_op jit(solution)/shard_map/all_to_all | solution.py:15
  505.4 7.6 %slice-start = ((s8[6291456]{0:T(1024)(128)(4,1)}), s8[4194304]{0:T(1024)(128)(4,1)S(1)}, s32[]{:S(2)}) async-start(s8[6291456]{0:T(1024)(128)(4,1)} %bitcast.34), calls=%async_computation.16 | async-start | bytes 8388608
  506.9 6.1 %slice-start.1 = ((s8[6291456]{0:T(1024)(128)(4,1)}), s8[2097152]{0:T(1024)(128)(4,1)S(1)}, s32[]{:S(2)}) async-start(s8[6291456]{0:T(1024)(128)(4,1)} %bitcast.34), calls=%async_computation.17 | async-start | bytes 4194304
Sparse Core Ops, SparseCore 0:
  85.6 57.7 all-gather.6
  165.4 61.2 all-gather.8
  228.8 46.1 all-gather.10
  276.5 50.4 all-gather.12
  338.9 44.6 all-gather.14
  385.7 46.3 all-gather.16
where the time goes:
time: 532 us; the launch traced here: 523 us
  blocking collectives  365 us (69%)
  local copies, waits for them, and re-layouts  74 us (14%)
  waiting for transfers between devices  29.1 us (5%)
  matrix products  16.4 us (3%)
  other arithmetic  16.1 us (3%)
  between operations  14.8 us (3%)
  starting transfers between devices  7.57 us (1%)
    all_to_all x4, blocking collectives, regroup(): lax.all_to_all(spread, 'fs', split_axis=1, concat_axis=0, tiled=True)  172 us
    all_to_all x4, blocking collectives, regroup(): lax.all_to_all(folded, 'tp', split_axis=0, concat_axis=1, tiled=True)  126 us
    all_gather x2, blocking collectives, sum_over_hidden(): return lax.all_gather(summed, 'fs', axis=1, tiled=True).astype(jnp.float32)  67.3 us
    all_gather x4, local copies, waits for them, and re-layouts, regroup(): whole = lax.all_gather(owned, 'tp', axis=1, tiled=True)  36.9 us
    all_to_all x2, waiting for transfers between devices, sum_over_hidden(): lax.all_to_all(partial_value.astype(jnp.bfloat16), 'fs', split_axis=1, co...  28.4 us
    all_to_all x12, local copies, waits for them, and re-layouts, regroup(): lax.all_to_all(spread, 'fs', split_axis=1, concat_axis=0, tiled=True)  18.8 us
    dot_general x2, matrix products, half_step(): partial_value = jnp.dot(hidden, w_down, preferred_element_type=jnp.float32)  13.9 us
  transfers between devices with their start and end apart: 8, of which 3 were waited for; matrix products, arithmetic and copies ran while one was open for 14% of the time, Pallas kernels for 0%

commit v1 on v0

--- a/solution.py
+++ b/solution.py
@@ -2,6 +2,12 @@
 import jax.numpy as jnp
 from jax import lax
 from jax.sharding import PartitionSpec as P
+
+
+def gather_blocks(x, mesh_axis, dim):
+    parts = lax.all_gather(x, mesh_axis, axis=0, tiled=False)
+    whole = jnp.concatenate(parts, axis=dim)
+    return whole
 
 
 def plain_norm(values):
@@ -18,7 +24,7 @@
     rows = partial_value.shape[0]
     pieces = pieces.reshape(-1, rows, pieces.shape[1]).astype(jnp.float32)
     summed = jnp.sum(pieces, axis=0).astype(jnp.bfloat16)
-    return lax.all_gather(summed, "fs", axis=1, tiled=True).astype(jnp.float32)
+    return gather_blocks(summed, "fs", 1).astype(jnp.float32)
 
 
 def regroup(folded):

time: 532 us -> 529 us (level)
    all_to_all x4, blocking collectives: 172 us -> 164 us  [regroup(): lax.all_to_all(spread, 'fs', split_axis=1, concat_axis=0, tiled=True)]
    all_to_all x4, blocking collectives: 126 us -> 132 us  [regroup(): lax.all_to_all(folded, 'tp', split_axis=0, concat_axis=1, tiled=True)]
where the time goes in v1:
time: 529 us; the launch traced here: 520 us
  blocking collectives  362 us (68%)
  local copies, waits for them, and re-layouts  73.3 us (14%)
  waiting for transfers between devices  30.2 us (6%)
  matrix products  16.5 us (3%)
  other arithmetic  15.7 us (3%)
  between operations  14.7 us (3%)
  starting transfers between devices  7.89 us (1%)
    all_to_all x4, blocking collectives, regroup(): lax.all_to_all(spread, 'fs', split_axis=1, concat_axis=0, tiled=True)  164 us
    all_to_all x4, blocking collectives, regroup(): lax.all_to_all(folded, 'tp', split_axis=0, concat_axis=1, tiled=True)  132 us
    all_gather x2, blocking collectives, gather_blocks(): parts = lax.all_gather(x, mesh_axis, axis=0, tiled=False)  65.9 us
    all_gather x4, local copies, waits for them, and re-layouts, regroup(): whole = lax.all_gather(owned, 'tp', axis=1, tiled=True)  36.6 us
    all_to_all x2, waiting for transfers between devices, sum_over_hidden(): lax.all_to_all(partial_value.astype(jnp.bfloat16), 'fs', split_axis=1, co...  28.9 us
    all_to_all x12, local copies, waits for them, and re-layouts, regroup(): lax.all_to_all(spread, 'fs', split_axis=1, concat_axis=0, tiled=True)  18.8 us
    dot_general x2, matrix products, half_step(): partial_value = jnp.dot(hidden, w_down, preferred_element_type=jnp.float32)  14 us
  transfers between devices with their start and end apart: 8, of which 3 were waited for; matrix products, arithmetic and copies ran while one was open for 14% of the time, Pallas kernels for 0%

profile of v1, /device:TPU:0, one launch (start us, length us, event | category | flops | bytes accessed | tf_op | source)
XLA Modules:
  0.0 520.1 jit_solution(5651162563330914459)
XLA Ops:
  8.0 3.7 multiply_convert_fusion.3
  11.7 24.1 %all_to_all.154 = bf16[4,96,2048]{2,1,0:T(8,128)(2,1)S(1)} all-to-all(bf16[4,96,2048]{2,1,0:T(8,128)(2,1)S(1)} %bitcast.66), channel_id=1, replica_groups=mesh['fs'=8,'tp'=4] {'tp'}, dimensions={0} | all-to-all | bytes 3145728 | tf_op jit(solution)/shard_map/all_to_all | solution.py:31
  37.0 1.8 all_to_all.119
  38.9 2.3 copy.31
  41.2 42.3 %all_to_all.155 = bf16[96,8,1024]{2,0,1:T(8,128)(2,1)S(1)} all-to-all(bf16[96,8,1024]{2,0,1:T(8,128)(2,1)S(1)} %copy.31), channel_id=1, replica_groups=mesh['fs'=8,'tp'=4] {'fs'}, dimensions={1} | all-to-all | bytes 3145728 | tf_op jit(solution)/shard_map/all_to_all | solution.py:34
  83.5 2.0 copy.32
  85.6 36.1 %all_to_all.156 = bf16[4,96,2048]{2,1,0:T(8,128)(2,1)S(1)} all-to-all(bf16[4,96,2048]{2,1,0:T(8,128)(2,1)S(1)} %bitcast.64), channel_id=1, replica_groups=mesh['fs'=8,'tp'=4] {'tp'}, dimensions={0} | all-to-all | bytes 3145728 | tf_op jit(solution)/shard_map/all_to_all | solution.py:31
  124.2 39.1 %all_to_all.157 = bf16[96,8,1024]{2,0,1:T(8,128)(2,1)S(1)} all-to-all(bf16[96,8,1024]{2,0,1:T(8,128)(2,1)S(1)} %copy.35), channel_id=1, replica_groups=mesh['fs'=8,'tp'=4] {'fs'}, dimensions={1} | all-to-all | bytes 3145728 | tf_op jit(solution)/shard_map/all_to_all | solution.py:34
  163.3 2.0 copy.36
  166.8 3.9 multiply_convert_fusion.1
  170.7 39.8 %all_to_all.158 = bf16[4,96,2048]{2,1,0:T(8,128)(2,1)S(1)} all-to-all(bf16[4,96,2048]{2,1,0:T(8,128)(2,1)S(1)} %bitcast.67), channel_id=1, replica_groups=mesh['fs'=8,'tp'=4] {'tp'}, dimensions={0} | all-to-all | bytes 3145728 | tf_op jit(solution)/shard_map/all_to_all | solution.py:31
  211.7 1.8 all_to_all.133
  213.6 2.3 copy.41
  215.8 40.1 %all_to_all.159 = bf16[96,8,1024]{2,0,1:T(8,128)(2,1)S(1)} all-to-all(bf16[96,8,1024]{2,0,1:T(8,128)(2,1)S(1)} %copy.41), channel_id=1, replica_groups=mesh['fs'=8,'tp'=4] {'fs'}, dimensions={1} | all-to-all | bytes 3145728 | tf_op jit(solution)/shard_map/all_to_all | solution.py:34
  255.9 2.0 copy.42
  258.0 32.2 %all_to_all.160 = bf16[4,96,2048]{2,1,0:T(8,128)(2,1)S(1)} all-to-all(bf16[4,96,2048]{2,1,0:T(8,128)(2,1)S(1)} %bitcast.65), channel_id=1, replica_groups=mesh['fs'=8,'tp'=4] {'tp'}, dimensions={0} | all-to-all | bytes 3145728 | tf_op jit(solution)/shard_map/all_to_all | solution.py:31
  292.7 42.4 %all_to_all.161 = bf16[96,8,1024]{2,0,1:T(8,128)(2,1)S(1)} all-to-all(bf16[96,8,1024]{2,0,1:T(8,128)(2,1)S(1)} %copy.45), channel_id=1, replica_groups=mesh['fs'=8,'tp'=4] {'fs'}, dimensions={1} | all-to-all | bytes 3145728 | tf_op jit(solution)/shard_map/all_to_all | solution.py:34
  335.1 2.0 copy.46
  340.4 9.4 %copy.33 = bf16[8,384,1024]{2,1,0:T(8,128)(2,1)} copy(bf16[8,384,1024]{2,0,1:T(8,128)(2,1)} %all-gather.9.cloned.1.call-done) | data formatting | bytes 12582912 | tf_op jit(solution)/shard_map/all_gather | solution.py:36
  349.8 9.1 %copy.37 = bf16[8,384,1024]{2,1,0:T(8,128)(2,1)} copy(bf16[8,384,1024]{2,0,1:T(8,128)(2,1)} %all-gather.11.cloned.1.call-done) | data formatting | bytes 12582912 | tf_op jit(solution)/shard_map/all_gather | solution.py:36
  360.2 7.1 %convolution_convert_fusion.1 = bf16[160,3072]{1,0:T(8,128)(2,1)S(1)} fusion(bf16[1024,3072]{1,0:T(8,128)(2,1)} %all-gather.13.cloned.1.call-done, bf16[3072,1024]{1,0:T(8,128)(2,1)} %bitcast.60, f32[160,1024]{1,0:T(8,128)S(1)} %fusion.14, bf16[160,3072]{1,0:T(8,128)(2,1)S(1)} %copy-done, f32[160]{0:T(256)S(1)} %add_rsqrt_fusion.2, ...), kind=kOutput, calls=%fused_computation.1 | convolution fusion | flops 2016706560 | bytes 15205632 | tf_op jit(solution)/shard_map/dot_general | solution.py:44
  368.4 4.1 all-to-all-start.4
  372.5 9.1 %copy.43 = bf16[8,384,1024]{2,1,0:T(8,128)(2,1)} copy(bf16[8,384,1024]{2,0,1:T(8,128)(2,1)} %all-gather.15.cloned.1.call-done) | data formatting | bytes 12582912 | tf_op jit(solution)/shard_map/all_gather | solution.py:36
  382.6 9.0 %copy.47 = bf16[8,384,1024]{2,1,0:T(8,128)(2,1)} copy(bf16[8,384,1024]{2,0,1:T(8,128)(2,1)} %all-gather.17.cloned.1.call-done) | data formatting | bytes 12582912 | tf_op jit(solution)/shard_map/all_gather | solution.py:36
  391.6 5.1 all-to-all-done.4
  396.9 33.0 %all-gather = bf16[1280,384]{1,0:T(8,128)(2,1)S(1)} all-gather(bf16[160,384]{1,0:T(8,128)(2,1)S(1)} %reduce_sum.80), channel_id=2, replica_groups=mesh['fs'=8,'tp'=4] {'fs'}, dimensions={0}, use_global_device_ids=true | all-gather | bytes 1105920 | tf_op jit(solution)/shard_map/all_gather | solution.py:8
  434.1 6.9 %convolution_convert_fusion = bf16[160,3072]{1,0:T(8,128)(2,1)S(1)} fusion(bf16[1024,3072]{1,0:T(8,128)(2,1)} %all-gather.19.cloned.1.call-done, bf16[160,3072]{1,0:T(8,128)(2,1)S(1)} %multiply_convert_fusion.5, bf16[3072,1024]{1,0:T(8,128)(2,1)} %bitcast.62, f32[160,1024]{1,0:T(8,128)S(1)} %fusion.16), kind=kOutput, calls=%fused_computation | convolution fusion | flops 2014740480 | bytes 15204352 | tf_op jit(solution)/shard_map/dot_general | solution.py:44
  442.1 3.6 all-to-all-start.9
  445.7 23.9 %all-to-all-done.9 = bf16[160,8,384]{2,0,1:T(8,128)(2,1)S(1)} async-done(((bf16[160,8,384]{2,0,1:T(8,128)(2,1)}), bf16[160,8,384]{2,0,1:T(8,128)(2,1)S(1)}, u32[]{:S(2)}, u32[]{:S(2)}) %all-to-all-start.9) | async-done | bytes 983072 | tf_op jit(solution)/shard_map/all_to_all | solution.py:21
  469.7 32.9 %all-gather.1 = bf16[1280,384]{1,0:T(8,128)(2,1)S(1)} all-gather(bf16[160,384]{1,0:T(8,128)(2,1)S(1)} %reduce_sum.83), channel_id=3, replica_groups=mesh['fs'=8,'tp'=4] {'fs'}, dimensions={0}, use_global_device_ids=true | all-gather | bytes 1105920 | tf_op jit(solution)/shard_map/all_gather | solution.py:8
  505.7 3.2 copy.60
  510.4 2.7 copy.61
  (83 shorter events, 26.6 us)
Async XLA Ops:
  7.2 333.2 %all-gather.9.cloned.1.call-start = ((), (), s32[]{:S(2)}) async-start(), calls=%async_computation.10 | async-start | bytes 7864320 | tf_op jit(solution)/shard_map/all_gather | solution.py:36
  85.5 264.3 %all-gather.11.cloned.1.call-start = ((), (), s32[]{:S(2)}) async-start(), calls=%async_computation.11 | async-start | bytes 7864320 | tf_op jit(solution)/shard_map/all_gather | solution.py:36
  163.3 2.1 copy-start.2
  165.3 1.4 copy-start.5
  165.3 194.9 %all-gather.13.cloned.1.call-start = ((), (), s32[]{:S(2)}) async-start(), calls=%async_computation.12 | async-start | bytes 7864320 | tf_op jit(solution)/shard_map/all_gather | solution.py:70
  166.7 205.8 %all-gather.15.cloned.1.call-start = ((), (), s32[]{:S(2)}) async-start(), calls=%async_computation.13 | async-start | bytes 7864320 | tf_op jit(solution)/shard_map/all_gather | solution.py:36
  258.0 124.7 %all-gather.17.cloned.1.call-start = ((), (), s32[]{:S(2)}) async-start(), calls=%async_computation.14 | async-start | bytes 7864320 | tf_op jit(solution)/shard_map/all_gather | solution.py:36
  335.1 2.1 copy-start.3
  337.1 97.0 %all-gather.19.cloned.1.call-start = ((), (), s32[]{:S(2)}) async-start(), calls=%async_computation.15 | async-start | bytes 7864320 | tf_op jit(solution)/shard_map/all_gather | solution.py:73
  338.5 1.2 copy-start
  349.8 9.2 %copy-start.1 = (bf16[8,384,1024]{2,1,0:T(8,128)(2,1)S(1)}, bf16[8,384,1024]{2,1,0:T(8,128)(2,1)}, u32[]{:S(2)}) copy-start(bf16[8,384,1024]{2,1,0:T(8,128)(2,1)} %copy.33) | copy-start | bytes 18874372
  367.3 5.1 copy-start.4
  368.4 28.3 %all-to-all-start.4 = ((bf16[160,8,384]{2,0,1:T(8,128)(2,1)}), bf16[160,8,384]{2,0,1:T(8,128)(2,1)S(1)}, u32[]{:S(2)}, u32[]{:S(2)}) async-start(bf16[160,8,384]{2,0,1:T(8,128)(2,1)} %bitcast.41), calls=%async_computation.4 | async-start | bytes 1966080 | tf_op jit(solution)/shard_map/all_to_all | solution.py:21
  429.9 2.4 slice-start
  430.2 2.6 slice-start.1
  442.1 27.4 %all-to-all-start.9 = ((bf16[160,8,384]{2,0,1:T(8,128)(2,1)}), bf16[160,8,384]{2,0,1:T(8,128)(2,1)S(1)}, u32[]{:S(2)}, u32[]{:S(2)}) async-start(bf16[160,8,384]{2,0,1:T(8,128)(2,1)} %bitcast.40), calls=%async_computation.9 | async-start | bytes 1966080 | tf_op jit(solution)/shard_map/all_to_all | solution.py:21
  502.5 2.7 slice-start.2
  502.9 2.9 slice-start.3
  503.8 5.2 slice-start.4
  505.7 4.6 slice-start.5
Sparse Core Ops, SparseCore 0:
  85.6 57.7 all-gather.8
  165.4 61.2 all-gather.10
  228.8 55.9 all-gather.12
  286.2 48.5 all-gather.14
  337.3 45.3 all-gather.16
  384.6 46.3 all-gather.18
